TPU v7x, 32 devices: a whole 2x2x4 slice. The times are simulated.
32 devices in a mesh: rep: 2 (over x), fs: 8 (over z, y), tp: 2 (over core).
Axes of the slice: x: 2, y: 2, z: 4, core: 2. Of those that a mesh axis runs over, the one named last changes fastest.
Arguments:
- tokens: bfloat16 [10240, 2048], P(('rep', 'fs'), 'tp'), may hold values from -6 to 6
- norm_first: float32 [2048], replicated, may hold values from 0.1 to 1.9
- norm_mix: float32 [2048], replicated, may hold values from 0.1 to 1.9
- norm_second: float32 [2048], replicated, may hold values from 0.1 to 1.9
- gate_weight: float32 [2048, 2816], P('fs', 'tp'), may hold values from -0.125 to 0.125
- up_weight: float32 [2048, 2816], P('fs', 'tp'), may hold values from -0.125 to 0.125
- down_weight: float32 [2816, 2048], P('tp', 'fs'), may hold values from -0.109375 to 0.109375
- gate_scale: float32 [2816], P('tp'), may hold values from 0.3 to 3
- up_scale: float32 [2816], P('tp'), may hold values from 0.3 to 3
- down_scale: float32 [2048], P('fs'), may hold values from 0.3 to 3
- u_weight: float32 [2048, 1024], P('fs', 'tp'), may hold values from -0.125 to 0.125
- v_weight: float32 [2048, 1024], P('fs', 'tp'), may hold values from -0.125 to 0.125
- u_scale: float32 [1024], P('tp'), may hold values from 0.3 to 3
- v_scale: float32 [1024], P('tp'), may hold values from 0.15 to 6
- ln_gain: float32 [1024], P('tp'), may hold values from 0.1 to 1.9
- ln_bias: float32 [1024], P('tp'), may hold values from -3 to 3
- spatial_weight: bfloat16 [8, 128, 128], P('tp'), may hold values from -0.25 to 0.25
- spatial_bias: float32 [8, 128], P('tp'), may hold values from 0.1 to 1.9
- out_weight: float32 [1024, 2048], P('tp', 'fs'), may hold values from -0.1875 to 0.1875
- out_scale: float32 [2048], P('fs'), may hold values from 0.3 to 3
Outputs:
- layer_out: bfloat16 [10240, 2048], P(('rep', 'fs'), 'tp')
All inputs are finite; a program needn't handle non-finite values.
Results may differ from a plain program's by a relative error of at most 0.019.
Values may be sent and summed in bfloat16 or wider, within the bound.
No kernel may reach another device: no remote copies, remote signals or barrier semaphores. Data moves between devices by JAX's collectives and lax.ppermute only.
A program may use at most 128 MiB of HBM per device.

v0:
```python
import jax
import jax.numpy as jnp
from jax import lax
from jax.sharding import PartitionSpec as P

BW = 1024
SPAN = 128
EPS = 1e-06


def add_pair(left, pieces):
    return (
        jnp.dot(left, pieces[0], preferred_element_type=jnp.float32),
        jnp.dot(left, pieces[1], preferred_element_type=jnp.float32),
    )


def on_device(
    tokens,
    norm_first,
    norm_mix,
    norm_second,
    gate_weight,
    up_weight,
    down_weight,
    gate_scale,
    up_scale,
    down_scale,
    u_weight,
    v_weight,
    u_scale,
    v_scale,
    ln_gain,
    ln_bias,
    spatial_weight,
    spatial_bias,
    out_weight,
    out_scale,
):
    wide_scales = (
        lax.all_gather(down_scale, "fs", axis=0, tiled=True),
        lax.all_gather(out_scale, "fs", axis=0, tiled=True),
    )
    gate_low = gate_weight.astype(jnp.bfloat16)
    up_low = up_weight.astype(jnp.bfloat16)
    down_low = down_weight.astype(jnp.bfloat16)
    count = tokens.shape[0]

    def full_norm(rows, gain):
        whole = lax.all_gather(rows, "tp", axis=1, tiled=True)
        values = whole.astype(jnp.float32)
        factor = lax.rsqrt(jnp.mean(values * values, axis=1, keepdims=True) + EPS)
        return (values * factor * gain).astype(jnp.bfloat16)

    def spread_sum(term):
        return lax.psum_scatter(
            term.astype(jnp.bfloat16), "tp", scatter_dimension=1, tiled=True
        ).astype(jnp.float32)

    gate_all, up_all = (
        lax.all_gather(gate_low, "fs", axis=0, tiled=True),
        lax.all_gather(up_low, "fs", axis=0, tiled=True),
    )

    def hidden_units(normed):
        gate = jnp.dot(normed, gate_all, preferred_element_type=jnp.float32) * gate_scale
        up_part = jnp.dot(normed, up_all, preferred_element_type=jnp.float32) * up_scale
        return (jax.nn.silu(gate) * up_part).astype(jnp.bfloat16)

    first_hidden = hidden_units(full_norm(tokens, norm_first))
    down_all = lax.all_gather(down_low, "fs", axis=1, tiled=True)
    first_term = (
        jnp.dot(first_hidden, down_all, preferred_element_type=jnp.float32) * wide_scales[0]
    )
    first = spread_sum(first_term)
    middle = (tokens.astype(jnp.float32) + 0.5 * first).astype(jnp.bfloat16)
    mix_normed = full_norm(middle, norm_mix)
    u_low = u_weight.astype(jnp.bfloat16)
    v_low = v_weight.astype(jnp.bfloat16)
    u_acc, v_acc = add_pair(
        mix_normed,
        (
            lax.all_gather(u_low, "fs", axis=0, tiled=True),
            lax.all_gather(v_low, "fs", axis=0, tiled=True),
        ),
    )
    u_pre = u_acc * u_scale
    v_act = jax.nn.gelu(v_acc * v_scale, approximate=True)
    totals = lax.psum((jnp.sum(v_act, axis=1), jnp.sum(v_act * v_act, axis=1)), "tp")
    v_mean = (totals[0] / BW)[:, None]
    v_var = (totals[1] / BW)[:, None] - v_mean * v_mean
    v_normed = ((v_act - v_mean) * lax.rsqrt(v_var + EPS) * ln_gain + ln_bias).astype(jnp.bfloat16)
    local_groups = spatial_weight.shape[0]
    channels = v_act.shape[1] // local_groups
    blocks = v_normed.reshape(count // SPAN, SPAN, local_groups, channels)
    lower = jnp.tril(jnp.ones((SPAN, SPAN), jnp.bool_))
    masked = jnp.where(lower[None], spatial_weight, jnp.zeros_like(spatial_weight))
    spatial = jnp.einsum("gts,nsgc->ntgc", masked, blocks, preferred_element_type=jnp.float32)
    spatial = spatial + spatial_bias.T[None, :, :, None]
    mixed = (jax.nn.gelu(u_pre, approximate=True) * spatial.reshape(count, v_act.shape[1])).astype(
        jnp.bfloat16
    )
    out_low = out_weight.astype(jnp.bfloat16)
    mix_term = (
        jnp.dot(
            mixed,
            lax.all_gather(out_low, "fs", axis=1, tiled=True),
            preferred_element_type=jnp.float32,
        )
        * wide_scales[1]
    )
    second = (middle.astype(jnp.float32) + spread_sum(mix_term)).astype(jnp.bfloat16)
    second_hidden = hidden_units(full_norm(second, norm_second))
    last = spread_sum(
        jnp.dot(second_hidden, down_all, preferred_element_type=jnp.float32) * wide_scales[0]
    )
    return (second.astype(jnp.float32) + 0.5 * last).astype(jnp.bfloat16)


def solution(mesh):
    placed = (
        P(("rep", "fs"), "tp"),
        P(),
        P(),
        P(),
        P("fs", "tp"),
        P("fs", "tp"),
        P("tp", "fs"),
        P("tp"),
        P("tp"),
        P("fs"),
        P("fs", "tp"),
        P("fs", "tp"),
        P("tp"),
        P("tp"),
        P("tp"),
        P("tp"),
        P("tp", None, None),
        P("tp", None),
        P("tp", "fs"),
        P("fs"),
    )
    return jax.shard_map(
        on_device, mesh=mesh, in_specs=placed, out_specs=P(("rep", "fs"), "tp"), check_vma=False
    )
```

profile of v0, /device:TPU:0, one launch (start us, length us, event | category | flops | bytes accessed | tf_op | source)
XLA Modules:
  0.0 577.7 jit_solution(11312762153509955955)
XLA Ops:
  6.5 0.7 all-gather.12.cloned.1.call-update
  7.3 0.0 all-gather.14.cloned.1.call-start
  7.3 2.4 convert_element_type.87
  9.8 0.0 all-gather.16.cloned.1.call-start
  9.8 0.9 convert_element_type.88
  10.8 0.0 all-gather.18.cloned.1.call-start
  10.9 0.9 convert_element_type.90
  11.8 0.0 reduce-scatter.4.cloned.1.call-start
  11.9 22.3 %all-gather = f32[8,1,256]{2,1,0:T(1,128)S(1)} all-gather(f32[1,1,256]{2,1,0:T(1,128)S(1)} %bitcast.34), channel_id=1, replica_groups=mesh['rep'=2,'fs'=8,'tp'=2] {'fs'}, dimensions={0}, use_global_device_ids=true | all-gather | bytes 9216 | tf_op jit(solution)/shard_map/all_gather | solution.py:41
  34.2 2.6 fusion
  36.9 81.8 %all-gather.14.cloned.1.call-done = bf16[2048,1408]{1,0:T(8,128)(2,1)} async-done(((bf16[256,1408]{1,0:T(8,128)(2,1)}), bf16[2048,1408]{1,0:T(8,128)(2,1)}) %all-gather.14.cloned.1.call-update) | async-done | bytes 5767184 | tf_op jit(solution)/shard_map/all_gather | solution.py:61
  118.7 8.7 %convolution_multiply_fusion.3 = f32[640,1408]{1,0:T(8,128)} fusion(bf16[2048,1408]{1,0:T(8,128)(2,1)} %all-gather.14.cloned.1.call-done, f32[1408]{0:T(1024)S(1)} %copy-done.19, bf16[640,2048]{1,0:T(8,128)(2,1)S(1)} %copy-done.4, f32[2048]{0:T(1024)S(1)} %copy-done.17, f32[640]{0:T(1024)S(1)} %add_rsqrt_fusion.3), kind=kOutput, calls=%fused_computation.23 | convolution fusion | flops 3697131520 | bytes 12009472 | tf_op jit(solution)/shard_map/dot_general | solution.py:66
  127.4 84.0 %all-gather.16.cloned.1.call-done = bf16[2048,1408]{1,0:T(8,128)(2,1)} async-done(((bf16[256,1408]{1,0:T(8,128)(2,1)}), bf16[2048,1408]{1,0:T(8,128)(2,1)}) %all-gather.16.cloned.1.call-update) | async-done | bytes 5767184 | tf_op jit(solution)/shard_map/all_gather | solution.py:62
  211.4 93.2 %all-gather.18.cloned.1.call-done = bf16[1408,2048]{1,0:T(8,128)(2,1)} async-done(((bf16[1408,256]{1,0:T(8,128)(2,1)}), bf16[1408,2048]{1,0:T(8,128)(2,1)}) %all-gather.18.cloned.1.call-update) | async-done | bytes 5767184 | tf_op jit(solution)/shard_map/all_gather | solution.py:71
  304.6 15.4 %multiply_convert_fusion.2 = bf16[640,2048]{1,0:T(8,128)(2,1)} fusion(bf16[1408,2048]{1,0:T(8,128)(2,1)} %all-gather.18.cloned.1.call-done, f32[2048]{0:T(1024)S(1)} %bitcast.30, bf16[2048,1408]{1,0:T(8,128)(2,1)} %all-gather.16.cloned.1.call-done, f32[640,1408]{1,0:T(8,128)} %convolution_multiply_fusion.3, f32[1408]{0:T(1024)S(1)} %copy-done.20, ...), kind=kOutput, calls=%fused_computation.17 | convolution fusion | flops 7396147200 | bytes 20406272 | tf_op jit(solution)/shard_map/dot_general | solution.py:73
  320.1 0.0 all-gather.20.cloned.1.call-start
  320.1 8.5 %reduce-scatter.4.cloned.1.call-done = bf16[640,1024]{1,0:T(8,128)(2,1)} async-done(((bf16[640,2048]{1,0:T(8,128)(2,1)}), bf16[640,1024]{1,0:T(8,128)(2,1)}) %reduce-scatter.4.cloned.1.call-update) | async-done | bytes 1310736 | tf_op jit(solution)/shard_map/reduce_scatter | solution.py:56
  328.7 2.9 add_convert_fusion.2
  331.6 0.0 all-gather.24.cloned.1.call-start
  331.7 0.7 convert_element_type.98
  332.5 0.0 all-gather.22.cloned.1.call-start
  332.5 0.7 convert_element_type.97
  333.3 0.0 all-gather.26.cloned.1.call-start
  333.3 0.7 convert_element_type.101
  334.1 0.0 reduce-scatter.6.cloned.1.call-start
  334.2 21.1 %all-gather.1 = f32[8,1,256]{2,1,0:T(1,128)S(1)} all-gather(f32[1,1,256]{2,1,0:T(1,128)S(1)} %bitcast.35), channel_id=1, replica_groups=mesh['rep'=2,'fs'=8,'tp'=2] {'fs'}, dimensions={0}, use_global_device_ids=true | all-gather | bytes 9216 | tf_op jit(solution)/shard_map/all_gather | solution.py:42
  355.3 2.6 fusion.3
  357.9 38.9 %all-gather.24.cloned.1.call-done = bf16[2048,512]{1,0:T(8,128)(2,1)} async-done(((bf16[256,512]{1,0:T(8,128)(2,1)}), bf16[2048,512]{1,0:T(8,128)(2,1)}) %all-gather.24.cloned.1.call-update) | async-done | bytes 2097168 | tf_op jit(solution)/shard_map/all_gather | solution.py:84
  396.8 4.6 fusion.57
  401.4 2.6 all-reduce
  404.1 1.6 add_convert_fusion.3
  405.7 0.2 reshape.55
  405.9 0.4 fusion.13
  406.3 1.0 copy.26
  407.3 39.3 %all-gather.22.cloned.1.call-done = bf16[2048,512]{1,0:T(8,128)(2,1)} async-done(((bf16[256,512]{1,0:T(8,128)(2,1)}), bf16[2048,512]{1,0:T(8,128)(2,1)}) %all-gather.22.cloned.1.call-update) | async-done | bytes 2097168 | tf_op jit(solution)/shard_map/all_gather | solution.py:83
  446.6 51.0 %all-gather.26.cloned.1.call-done = bf16[512,2048]{1,0:T(8,128)(2,1)} async-done(((bf16[512,256]{1,0:T(8,128)(2,1)}), bf16[512,2048]{1,0:T(8,128)(2,1)}) %all-gather.26.cloned.1.call-update) | async-done | bytes 2097168 | tf_op jit(solution)/shard_map/all_gather | solution.py:107
  497.6 7.8 %multiply_convert_fusion.1 = bf16[640,2048]{1,0:T(8,128)(2,1)} fusion(bf16[512,2048]{1,0:T(8,128)(2,1)} %all-gather.26.cloned.1.call-done, f32[2048]{0:T(1024)S(1)} %bitcast.32, f32[80,8,4,128]{3,2,1,0:T(4,128)S(1)} %bitcast.29, bf16[2048,512]{1,0:T(8,128)(2,1)} %all-gather.22.cloned.1.call-done, bf16[640,2048]{1,0:T(8,128)(2,1)} %all-gather.20.cloned.1.call-done, ...), kind=kOutput, calls=%fused_computation.16 | convolution fusion | flops 2695823360 | bytes 10768896 | tf_op jit(solution)/shard_map/dot_general | solution.py:105
  505.4 0.0 all-gather.28.cloned.1.call-start
  505.4 8.6 %reduce-scatter.6.cloned.1.call-done = bf16[640,1024]{1,0:T(8,128)(2,1)} async-done(((bf16[640,2048]{1,0:T(8,128)(2,1)}), bf16[640,1024]{1,0:T(8,128)(2,1)}) %reduce-scatter.6.cloned.1.call-update) | async-done | bytes 1310736 | tf_op jit(solution)/shard_map/reduce_scatter | solution.py:56
  514.0 2.9 add_convert_fusion.1
  516.9 0.3 reduce-scatter.8.cloned.1.call-start
  517.2 12.5 %all-gather.28.cloned.1.call-done = bf16[640,2048]{1,0:T(8,128)(2,1)} async-done(((bf16[640,1024]{1,0:T(8,128)(2,1)}), bf16[640,2048]{1,0:T(8,128)(2,1)}) %all-gather.28.cloned.1.call-update) | async-done | bytes 2621456 | tf_op jit(solution)/shard_map/all_gather | solution.py:50
  529.7 2.5 fusion.6
  532.2 0.0 copy-done.5
  532.2 8.7 %convolution_multiply_fusion.1 = f32[640,1408]{1,0:T(8,128)} fusion(bf16[2048,1408]{1,0:T(8,128)(2,1)} %all-gather.14.cloned.1.call-done, f32[1408]{0:T(1024)S(1)} %copy-done.19, bf16[640,2048]{1,0:T(8,128)(2,1)S(1)} %copy-done.5, f32[2048]{0:T(1024)S(1)} %copy-done.21, f32[640]{0:T(1024)S(1)} %add_rsqrt_fusion), kind=kOutput, calls=%fused_computation.20 | convolution fusion | flops 3697131520 | bytes 12009472 | tf_op jit(solution)/shard_map/dot_general | solution.py:66
  540.9 15.4 %multiply_convert_fusion = bf16[640,2048]{1,0:T(8,128)(2,1)} fusion(bf16[1408,2048]{1,0:T(8,128)(2,1)} %all-gather.18.cloned.1.call-done, f32[2048]{0:T(1024)S(1)} %bitcast.31, bf16[2048,1408]{1,0:T(8,128)(2,1)} %all-gather.16.cloned.1.call-done, f32[640,1408]{1,0:T(8,128)} %convolution_multiply_fusion.1, f32[1408]{0:T(1024)S(1)} %copy-done.20, ...), kind=kOutput, calls=%fused_computation.15 | convolution fusion | flops 7396147200 | bytes 20406272 | tf_op jit(solution)/shard_map/dot_general | solution.py:115
  556.3 11.6 %reduce-scatter.8.cloned.1.call-done = bf16[640,1024]{1,0:T(8,128)(2,1)} async-done(((bf16[640,2048]{1,0:T(8,128)(2,1)}), bf16[640,1024]{1,0:T(8,128)(2,1)}) %reduce-scatter.8.cloned.1.call-update) | async-done | bytes 1310736 | tf_op jit(solution)/shard_map/reduce_scatter | solution.py:56
  567.9 2.9 add_convert_fusion
  (66 shorter events, 0.4 us)
Async XLA Ops:
  6.5 3.3 copy-start.6
  6.5 27.7 %all-gather.12.cloned.1.call-start = ((), (), s32[]{:S(2)}) async-start(), calls=%async_computation.3 | async-start | bytes 3932160 | tf_op jit(solution)/shard_map/all_gather | solution.py:50
  7.3 3.6 copy-start.7
  7.3 111.4 %all-gather.14.cloned.1.call-start = ((), (), s32[]{:S(2)}) async-start(), calls=%async_computation.4 | async-start | bytes 6488064 | tf_op jit(solution)/shard_map/all_gather | solution.py:61
  9.8 2.1 copy-start.15
  9.8 201.6 %all-gather.16.cloned.1.call-start = ((), (), s32[]{:S(2)}) async-start(), calls=%async_computation.5 | async-start | bytes 6488064 | tf_op jit(solution)/shard_map/all_gather | solution.py:62
  10.8 107.9 %copy-start.17 = (f32[2048]{0:T(1024)S(1)}, f32[2048]{0:T(1024)}, u32[]{:S(2)}) copy-start(f32[2048]{0:T(1024)} %param.21) | copy-start | bytes 24580
  10.8 107.9 %copy-start.19 = (f32[1408]{0:T(1024)S(1)}, f32[1408]{0:T(1024)}, u32[]{:S(2)}) copy-start(f32[1408]{0:T(1024)} %param.27) | copy-start | bytes 16900
  10.8 293.8 %all-gather.18.cloned.1.call-start = ((), (), s32[]{:S(2)}) async-start(), calls=%async_computation.6 | async-start | bytes 6488064 | tf_op jit(solution)/shard_map/all_gather | solution.py:71
  11.8 316.8 %reduce-scatter.4.cloned.1.call-start = ((), (), s32[]{:S(2)}) async-start(), calls=%async_computation.7 | async-start | bytes 3932160 | tf_op jit(solution)/shard_map/reduce_scatter | solution.py:56
  34.2 84.5 %copy-start.4 = (bf16[640,2048]{1,0:T(8,128)(2,1)S(1)}, bf16[640,2048]{1,0:T(8,128)(2,1)}, u32[]{:S(2)}) copy-start(bf16[640,2048]{1,0:T(8,128)(2,1)} %all-gather.12.cloned.1.call-done) | copy-start | bytes 7864324
  36.9 267.8 %copy-start.20 = (f32[1408]{0:T(1024)S(1)}, f32[1408]{0:T(1024)}, u32[]{:S(2)}) copy-start(f32[1408]{0:T(1024)} %param.28) | copy-start | bytes 16900
  320.0 8.7 %copy-start.2 = (bf16[640,1024]{1,0:T(8,128)(2,1)S(1)}, bf16[640,1024]{1,0:T(8,128)(2,1)}, u32[]{:S(2)}) copy-start(bf16[640,1024]{1,0:T(8,128)(2,1)} %param.20) | copy-start | bytes 3932164
  320.1 11.6 %copy-start.8 = (f32[256,512]{1,0:T(8,128)S(1)}, f32[256,512]{1,0:T(8,128)}, u32[]{:S(2)}) copy-start(f32[256,512]{1,0:T(8,128)} %param.31) | copy-start | bytes 1572868
  320.1 12.5 %copy-start.9 = (f32[256,512]{1,0:T(8,128)S(1)}, f32[256,512]{1,0:T(8,128)}, u32[]{:S(2)}) copy-start(f32[256,512]{1,0:T(8,128)} %param.30) | copy-start | bytes 1572868
  320.1 35.2 %all-gather.20.cloned.1.call-start = ((), (), s32[]{:S(2)}) async-start(), calls=%async_computation.8 | async-start | bytes 3932160 | tf_op jit(solution)/shard_map/all_gather | solution.py:50
  331.6 1.7 copy-start.10
  331.6 2.5 copy-start.16
  331.6 65.2 %all-gather.24.cloned.1.call-start = ((), (), s32[]{:S(2)}) async-start(), calls=%async_computation.10 | async-start | bytes 2359296 | tf_op jit(solution)/shard_map/all_gather | solution.py:84
  332.4 64.4 %copy-start.18 = (f32[2048]{0:T(1024)S(1)}, f32[2048]{0:T(1024)}, u32[]{:S(2)}) copy-start(f32[2048]{0:T(1024)} %param.22) | copy-start | bytes 24580
  332.4 64.4 %copy-start.22 = (f32[512]{0:T(512)S(1)}, f32[512]{0:T(512)}, u32[]{:S(2)}) copy-start(f32[512]{0:T(512)} %param.33) | copy-start | bytes 6148
  332.5 114.1 %all-gather.22.cloned.1.call-start = ((), (), s32[]{:S(2)}) async-start(), calls=%async_computation.9 | async-start | bytes 2359296 | tf_op jit(solution)/shard_map/all_gather | solution.py:83
  333.3 164.3 %all-gather.26.cloned.1.call-start = ((), (), s32[]{:S(2)}) async-start(), calls=%async_computation.11 | async-start | bytes 2359296 | tf_op jit(solution)/shard_map/all_gather | solution.py:107
  334.1 179.9 %reduce-scatter.6.cloned.1.call-start = ((), (), s32[]{:S(2)}) async-start(), calls=%async_computation.12 | async-start | bytes 3932160 | tf_op jit(solution)/shard_map/reduce_scatter | solution.py:56
  355.3 41.5 %copy-start.3 = (bf16[640,2048]{1,0:T(8,128)(2,1)S(1)}, bf16[640,2048]{1,0:T(8,128)(2,1)}, u32[]{:S(2)}) copy-start(bf16[640,2048]{1,0:T(8,128)(2,1)} %all-gather.20.cloned.1.call-done) | copy-start | bytes 7864324
  357.9 46.2 %copy-start.13 = (f32[512]{0:T(512)S(1)}, f32[512]{0:T(512)}, u32[]{:S(2)}) copy-start(f32[512]{0:T(512)} %param.35) | copy-start | bytes 6148
  357.9 46.2 %copy-start.14 = (f32[512]{0:T(512)S(1)}, f32[512]{0:T(512)}, u32[]{:S(2)}) copy-start(f32[512]{0:T(512)} %param.34) | copy-start | bytes 6148
  401.4 4.4 copy-start.11
  401.4 4.5 copy-start.12
  405.9 91.7 %copy-start.23 = (f32[512]{0:T(512)S(1)}, f32[512]{0:T(512)}, u32[]{:S(2)}) copy-start(f32[512]{0:T(512)} %param.32) | copy-start | bytes 6148
  505.3 8.7 %copy-start = (bf16[640,1024]{1,0:T(8,128)(2,1)S(1)}, bf16[640,1024]{1,0:T(8,128)(2,1)}, u32[]{:S(2)}) copy-start(bf16[640,1024]{1,0:T(8,128)(2,1)} %add_convert_fusion.2) | copy-start | bytes 3932164
  505.4 24.4 %all-gather.28.cloned.1.call-start = ((), (), s32[]{:S(2)}) async-start(), calls=%async_computation.13 | async-start | bytes 3932160 | tf_op jit(solution)/shard_map/all_gather | solution.py:50
  516.9 15.3 %copy-start.21 = (f32[2048]{0:T(1024)S(1)}, f32[2048]{0:T(1024)}, u32[]{:S(2)}) copy-start(f32[2048]{0:T(1024)} %param.23) | copy-start | bytes 24580
  516.9 51.0 %reduce-scatter.8.cloned.1.call-start = ((), (), s32[]{:S(2)}) async-start(), calls=%async_computation.14 | async-start | bytes 3932160 | tf_op jit(solution)/shard_map/reduce_scatter | solution.py:56
  529.7 2.5 copy-start.5
  556.3 11.6 %copy-start.1 = (bf16[640,1024]{1,0:T(8,128)(2,1)S(1)}, bf16[640,1024]{1,0:T(8,128)(2,1)}, u32[]{:S(2)}) copy-start(bf16[640,1024]{1,0:T(8,128)(2,1)} %add_convert_fusion.1) | copy-start | bytes 3932164
Sparse Core Ops, SparseCore 0:
  8.9 14.0 all-gather.11
  25.2 93.4 all-gather.13
  120.9 90.4 all-gather.15
  213.3 91.2 all-gather.17
  320.2 8.4 reduce-scatter.3
  331.8 12.6 all-gather.19
  346.5 50.2 all-gather.23
  399.0 47.6 all-gather.21
  448.7 48.8 all-gather.25
  505.5 8.4 reduce-scatter.5
  517.0 12.6 all-gather.27
  556.4 11.4 reduce-scatter.7
where the time goes:
time: 578 us
  waiting for transfers between devices  430 us (74%)
  matrix products  60.8 us (11%)
  blocking collectives  46 us (8%)
  other arithmetic  24.6 us (4%)
  between operations  13.8 us (2%)
    all_gather x1, waiting for transfers between devices, on_device(): down_all = lax.all_gather(down_low, 'fs', axis=1, tiled=True)  93.2 us
    all_gather x1, waiting for transfers between devices, on_device(): lax.all_gather(up_low, 'fs', axis=0, tiled=True)  84 us
    all_gather x1, waiting for transfers between devices, on_device(): lax.all_gather(gate_low, 'fs', axis=0, tiled=True)  81.8 us
    all_gather x1, waiting for transfers between devices, on_device(): lax.all_gather(out_low, 'fs', axis=1, tiled=True)  51 us
    all_gather x1, waiting for transfers between devices, on_device(): lax.all_gather(u_low, 'fs', axis=0, tiled=True)  39.3 us
    all_gather x1, waiting for transfers between devices, on_device(): lax.all_gather(v_low, 'fs', axis=0, tiled=True)  38.9 us
    reduce_scatter x3, waiting for transfers between devices, spread_sum(): lax.psum_scatter(term.astype(jnp.bfloat16), 'tp', scatter_dimension=1, ti...  28.7 us
    all_gather x1, blocking collectives, on_device(): lax.all_gather(down_scale, 'fs', axis=0, tiled=True)  22.3 us
  transfers between devices with their start and end apart: 12, of which 10 were waited for; matrix products, arithmetic and copies ran while one was open for 5% of the time, Pallas kernels for 0%

commit v1 on v0

--- a/solution.py
+++ b/solution.py
@@ -6,6 +6,7 @@
 BW = 1024
 SPAN = 128
 EPS = 1e-06
+_list_region = lambda panel, mesh_dim: jnp.concatenate(lax.all_gather(panel, mesh_dim), axis=1)
 
 
 def add_pair(left, pieces):
@@ -102,11 +103,7 @@
     )
     out_low = out_weight.astype(jnp.bfloat16)
     mix_term = (
-        jnp.dot(
-            mixed,
-            lax.all_gather(out_low, "fs", axis=1, tiled=True),
-            preferred_element_type=jnp.float32,
-        )
+        jnp.dot(mixed, _list_region(out_low, "fs"), preferred_element_type=jnp.float32)
         * wide_scales[1]
     )
     second = (middle.astype(jnp.float32) + spread_sum(mix_term)).astype(jnp.bfloat16)

time: 578 us -> 576 us (level)
  waiting for transfers between devices: 430 us -> 423 us
    all_gather x1, waiting for transfers between devices: 51 us -> 26.7 us  [lax.all_gather(panel, mesh_dim)]
    all_gather x1, waiting for transfers between devices: 38.9 us -> 49.9 us  [on_device(): lax.all_gather(v_low, 'fs', axis=0, tiled=True)]
    all_gather x3, waiting for transfers between devices: 12.5 us -> 20 us  [full_norm(): whole = lax.all_gather(rows, 'tp', axis=1, tiled=True)]
  transfers between devices with their start and end apart: 12 -> 12, of which waited for: 10 -> 11; matrix products, arithmetic and copies ran while one was open for 5% -> 6% of each run, Pallas kernels for 0% -> 0%
where the time goes in v1:
time: 576 us; the launch traced here: 575 us
  waiting for transfers between devices  423 us (73%)
  matrix products  60.9 us (11%)
  blocking collectives  46 us (8%)
  other arithmetic  24.5 us (4%)
  between operations  13.8 us (2%)
  local copies, waits for them, and re-layouts  6.19 us (1%)
    all_gather x1, waiting for transfers between devices, on_device(): down_all = lax.all_gather(down_low, 'fs', axis=1, tiled=True)  93.2 us
    all_gather x1, waiting for transfers between devices, on_device(): lax.all_gather(up_low, 'fs', axis=0, tiled=True)  84 us
    all_gather x1, waiting for transfers between devices, on_device(): lax.all_gather(gate_low, 'fs', axis=0, tiled=True)  81.8 us
    all_gather x1, waiting for transfers between devices, on_device(): lax.all_gather(v_low, 'fs', axis=0, tiled=True)  49.9 us
    all_gather x1, waiting for transfers between devices, on_device(): lax.all_gather(u_low, 'fs', axis=0, tiled=True)  39.2 us
    reduce_scatter x3, waiting for transfers between devices, spread_sum(): lax.psum_scatter(term.astype(jnp.bfloat16), 'tp', scatter_dimension=1, ti...  27.3 us
    all_gather x1, waiting for transfers between devices, lax.all_gather(panel, mesh_dim)  26.7 us
    all_gather x1, blocking collectives, on_device(): lax.all_gather(down_scale, 'fs', axis=0, tiled=True)  22.3 us
  transfers between devices with their start and end apart: 12, of which 11 were waited for; matrix products, arithmetic and copies ran while one was open for 6% of the time, Pallas kernels for 0%

profile of v1, /device:TPU:0, one launch (start us, length us, event | category | flops | bytes accessed | tf_op | source)
XLA Modules:
  0.0 575.2 jit_solution(9255359540649770675)
XLA Ops:
  6.5 0.7 all-gather.13.cloned.1.call-update
  7.3 2.4 convert_element_type.87
  9.8 0.0 all-gather.17.cloned.1.call-start
  9.8 0.9 convert_element_type.88
  10.8 0.0 all-gather.19.cloned.1.call-start
  10.9 0.9 convert_element_type.90
  11.8 0.0 reduce-scatter.4.cloned.1.call-start
  11.9 22.3 %all-gather.1 = f32[8,1,256]{2,1,0:T(1,128)S(1)} all-gather(f32[1,1,256]{2,1,0:T(1,128)S(1)} %bitcast.40), channel_id=1, replica_groups=mesh['rep'=2,'fs'=8,'tp'=2] {'fs'}, dimensions={0}, use_global_device_ids=true | all-gather | bytes 9216 | tf_op jit(solution)/shard_map/all_gather | solution.py:42
  34.2 2.6 fusion
  36.9 81.8 %all-gather.15.cloned.1.call-done = bf16[2048,1408]{1,0:T(8,128)(2,1)} async-done(((bf16[256,1408]{1,0:T(8,128)(2,1)}), bf16[2048,1408]{1,0:T(8,128)(2,1)}) %all-gather.15.cloned.1.call-update) | async-done | bytes 5767184 | tf_op jit(solution)/shard_map/all_gather | solution.py:62
  118.7 8.7 %convolution_multiply_fusion.3 = f32[640,1408]{1,0:T(8,128)} fusion(bf16[2048,1408]{1,0:T(8,128)(2,1)} %all-gather.15.cloned.1.call-done, f32[1408]{0:T(1024)S(1)} %copy-done.19, bf16[640,2048]{1,0:T(8,128)(2,1)S(1)} %copy-done.4, f32[2048]{0:T(1024)S(1)} %copy-done.17, f32[640]{0:T(1024)S(1)} %add_rsqrt_fusion.3), kind=kOutput, calls=%fused_computation.23 | convolution fusion | flops 3697131520 | bytes 12009472 | tf_op jit(solution)/shard_map/dot_general | solution.py:67
  127.4 84.0 %all-gather.17.cloned.1.call-done = bf16[2048,1408]{1,0:T(8,128)(2,1)} async-done(((bf16[256,1408]{1,0:T(8,128)(2,1)}), bf16[2048,1408]{1,0:T(8,128)(2,1)}) %all-gather.17.cloned.1.call-update) | async-done | bytes 5767184 | tf_op jit(solution)/shard_map/all_gather | solution.py:63
  211.4 93.2 %all-gather.19.cloned.1.call-done = bf16[1408,2048]{1,0:T(8,128)(2,1)} async-done(((bf16[1408,256]{1,0:T(8,128)(2,1)}), bf16[1408,2048]{1,0:T(8,128)(2,1)}) %all-gather.19.cloned.1.call-update) | async-done | bytes 5767184 | tf_op jit(solution)/shard_map/all_gather | solution.py:72
  304.6 15.4 %multiply_convert_fusion.2 = bf16[640,2048]{1,0:T(8,128)(2,1)} fusion(bf16[1408,2048]{1,0:T(8,128)(2,1)} %all-gather.19.cloned.1.call-done, f32[2048]{0:T(1024)S(1)} %bitcast.36, bf16[2048,1408]{1,0:T(8,128)(2,1)} %all-gather.17.cloned.1.call-done, f32[640,1408]{1,0:T(8,128)} %convolution_multiply_fusion.3, f32[1408]{0:T(1024)S(1)} %copy-done.20, ...), kind=kOutput, calls=%fused_computation.17 | convolution fusion | flops 7396147200 | bytes 20406272 | tf_op jit(solution)/shard_map/dot_general | solution.py:74
  320.1 0.0 all-gather.29.cloned.1.call-start
  320.1 1.0 copy-done.8
  321.1 0.7 convert_element_type.101
  321.9 0.0 all-gather.21.cloned.1.call-start
  321.9 6.8 %reduce-scatter.4.cloned.1.call-done = bf16[640,1024]{1,0:T(8,128)(2,1)} async-done(((bf16[640,2048]{1,0:T(8,128)(2,1)}), bf16[640,1024]{1,0:T(8,128)(2,1)}) %reduce-scatter.4.cloned.1.call-update) | async-done | bytes 1310736 | tf_op jit(solution)/shard_map/reduce_scatter | solution.py:57
  328.7 2.9 add_convert_fusion.2
  331.6 0.0 all-gather.25.cloned.1.call-start
  331.7 0.7 convert_element_type.98
  332.5 0.0 all-gather.23.cloned.1.call-start
  332.5 0.7 convert_element_type.97
  333.3 0.0 reduce-scatter.6.cloned.1.call-start
  333.4 21.1 %all-gather.2 = f32[8,1,256]{2,1,0:T(1,128)S(1)} all-gather(f32[1,1,256]{2,1,0:T(1,128)S(1)} %bitcast.41), channel_id=1, replica_groups=mesh['rep'=2,'fs'=8,'tp'=2] {'fs'}, dimensions={0}, use_global_device_ids=true | all-gather | bytes 9216 | tf_op jit(solution)/shard_map/all_gather | solution.py:43
  354.5 26.7 %all-gather.29.cloned.1.call-done = bf16[4096,256]{1,0:T(8,128)(2,1)} async-done(((bf16[512,256]{1,0:T(8,128)(2,1)}), bf16[4096,256]{1,0:T(8,128)(2,1)}) %all-gather.29.cloned.1.call-update) | async-done | bytes 2097168 | tf_op jit(solution)/shard_map/all_gather | solution.py:9
  381.2 3.9 copy.34
  385.1 7.5 %all-gather.21.cloned.1.call-done = bf16[640,2048]{1,0:T(8,128)(2,1)} async-done(((bf16[640,1024]{1,0:T(8,128)(2,1)}), bf16[640,2048]{1,0:T(8,128)(2,1)}) %all-gather.21.cloned.1.call-update) | async-done | bytes 2621456 | tf_op jit(solution)/shard_map/all_gather | solution.py:51
  392.6 2.5 fusion.3
  395.1 49.9 %all-gather.25.cloned.1.call-done = bf16[2048,512]{1,0:T(8,128)(2,1)} async-done(((bf16[256,512]{1,0:T(8,128)(2,1)}), bf16[2048,512]{1,0:T(8,128)(2,1)}) %all-gather.25.cloned.1.call-update) | async-done | bytes 2097168 | tf_op jit(solution)/shard_map/all_gather | solution.py:85
  445.0 4.7 fusion.57
  449.7 2.6 all-reduce
  452.3 1.6 add_convert_fusion.3
  454.0 0.2 reshape.61
  454.2 0.4 fusion.13
  454.6 1.0 copy.33
  455.6 39.2 %all-gather.23.cloned.1.call-done = bf16[2048,512]{1,0:T(8,128)(2,1)} async-done(((bf16[256,512]{1,0:T(8,128)(2,1)}), bf16[2048,512]{1,0:T(8,128)(2,1)}) %all-gather.23.cloned.1.call-update) | async-done | bytes 2097168 | tf_op jit(solution)/shard_map/all_gather | solution.py:84
  494.8 7.7 %multiply_convert_fusion.1 = bf16[640,2048]{1,0:T(8,128)(2,1)} fusion(bf16[512,2048]{0,1:T(8,128)(2,1)} %bitcast.34, f32[2048]{0:T(1024)S(1)} %bitcast.38, f32[80,8,4,128]{3,2,1,0:T(4,128)S(1)} %bitcast.35, bf16[2048,512]{1,0:T(8,128)(2,1)} %all-gather.23.cloned.1.call-done, bf16[640,2048]{1,0:T(8,128)(2,1)} %all-gather.21.cloned.1.call-done, ...), kind=kOutput, calls=%fused_computation.16 | convolution fusion | flops 2695823360 | bytes 10768896 | tf_op jit(solution)/shard_map/dot_general | solution.py:106
  502.6 8.9 %reduce-scatter.6.cloned.1.call-done = bf16[640,1024]{1,0:T(8,128)(2,1)} async-done(((bf16[640,2048]{1,0:T(8,128)(2,1)}), bf16[640,1024]{1,0:T(8,128)(2,1)}) %reduce-scatter.6.cloned.1.call-update) | async-done | bytes 1310736 | tf_op jit(solution)/shard_map/reduce_scatter | solution.py:57
  511.6 2.9 add_convert_fusion.1
  514.5 0.3 reduce-scatter.8.cloned.1.call-start
  514.8 12.5 %all-gather.27.cloned.1.call-done = bf16[640,2048]{1,0:T(8,128)(2,1)} async-done(((bf16[640,1024]{1,0:T(8,128)(2,1)}), bf16[640,2048]{1,0:T(8,128)(2,1)}) %all-gather.27.cloned.1.call-update) | async-done | bytes 2621456 | tf_op jit(solution)/shard_map/all_gather | solution.py:51
  527.3 2.5 fusion.6
  529.8 8.7 %convolution_multiply_fusion.1 = f32[640,1408]{1,0:T(8,128)} fusion(bf16[2048,1408]{1,0:T(8,128)(2,1)} %all-gather.15.cloned.1.call-done, f32[1408]{0:T(1024)S(1)} %copy-done.19, bf16[640,2048]{1,0:T(8,128)(2,1)S(1)} %copy-done.5, f32[2048]{0:T(1024)S(1)} %copy-done.21, f32[640]{0:T(1024)S(1)} %add_rsqrt_fusion), kind=kOutput, calls=%fused_computation.20 | convolution fusion | flops 3697131520 | bytes 12009472 | tf_op jit(solution)/shard_map/dot_general | solution.py:67
  538.4 15.4 %multiply_convert_fusion = bf16[640,2048]{1,0:T(8,128)(2,1)} fusion(bf16[1408,2048]{1,0:T(8,128)(2,1)} %all-gather.19.cloned.1.call-done, f32[2048]{0:T(1024)S(1)} %bitcast.37, bf16[2048,1408]{1,0:T(8,128)(2,1)} %all-gather.17.cloned.1.call-done, f32[640,1408]{1,0:T(8,128)} %convolution_multiply_fusion.1, f32[1408]{0:T(1024)S(1)} %copy-done.20, ...), kind=kOutput, calls=%fused_computation.15 | convolution fusion | flops 7396147200 | bytes 20406272 | tf_op jit(solution)/shard_map/dot_general | solution.py:112
  553.8 11.6 %reduce-scatter.8.cloned.1.call-done = bf16[640,1024]{1,0:T(8,128)(2,1)} async-done(((bf16[640,2048]{1,0:T(8,128)(2,1)}), bf16[640,1024]{1,0:T(8,128)(2,1)}) %reduce-scatter.8.cloned.1.call-update) | async-done | bytes 1310736 | tf_op jit(solution)/shard_map/reduce_scatter | solution.py:57
  565.5 2.9 add_convert_fusion
  (67 shorter events, 0.5 us)
Async XLA Ops:
  6.5 3.3 copy-start.6
  6.5 27.7 %all-gather.13.cloned.1.call-start = ((), (), s32[]{:S(2)}) async-start(), calls=%async_computation.3 | async-start | bytes 3932160 | tf_op jit(solution)/shard_map/all_gather | solution.py:51
  7.3 3.6 copy-start.7
  7.3 111.4 %all-gather.15.cloned.1.call-start = ((), (), s32[]{:S(2)}) async-start(), calls=%async_computation.4 | async-start | bytes 6488064 | tf_op jit(solution)/shard_map/all_gather | solution.py:62
  9.8 2.1 copy-start.15
  9.8 201.6 %all-gather.17.cloned.1.call-start = ((), (), s32[]{:S(2)}) async-start(), calls=%async_computation.5 | async-start | bytes 6488064 | tf_op jit(solution)/shard_map/all_gather | solution.py:63
  10.8 107.9 %copy-start.17 = (f32[2048]{0:T(1024)S(1)}, f32[2048]{0:T(1024)}, u32[]{:S(2)}) copy-start(f32[2048]{0:T(1024)} %param.21) | copy-start | bytes 24580
  10.8 107.9 %copy-start.19 = (f32[1408]{0:T(1024)S(1)}, f32[1408]{0:T(1024)}, u32[]{:S(2)}) copy-start(f32[1408]{0:T(1024)} %param.27) | copy-start | bytes 16900
  10.8 293.8 %all-gather.19.cloned.1.call-start = ((), (), s32[]{:S(2)}) async-start(), calls=%async_computation.6 | async-start | bytes 6488064 | tf_op jit(solution)/shard_map/all_gather | solution.py:72
  11.8 316.8 %reduce-scatter.4.cloned.1.call-start = ((), (), s32[]{:S(2)}) async-start(), calls=%async_computation.7 | async-start | bytes 3932160 | tf_op jit(solution)/shard_map/reduce_scatter | solution.py:57
  34.2 84.5 %copy-start.4 = (bf16[640,2048]{1,0:T(8,128)(2,1)S(1)}, bf16[640,2048]{1,0:T(8,128)(2,1)}, u32[]{:S(2)}) copy-start(bf16[640,2048]{1,0:T(8,128)(2,1)} %all-gather.13.cloned.1.call-done) | copy-start | bytes 7864324
  36.9 267.8 %copy-start.20 = (f32[1408]{0:T(1024)S(1)}, f32[1408]{0:T(1024)}, u32[]{:S(2)}) copy-start(f32[1408]{0:T(1024)} %param.28) | copy-start | bytes 16900
  320.0 1.0 copy-start.8
  320.0 8.7 %copy-start.2 = (bf16[640,1024]{1,0:T(8,128)(2,1)S(1)}, bf16[640,1024]{1,0:T(8,128)(2,1)}, u32[]{:S(2)}) copy-start(bf16[640,1024]{1,0:T(8,128)(2,1)} %param.20) | copy-start | bytes 3932164
  320.1 61.1 %all-gather.29.cloned.1.call-start = ((), (), s32[]{:S(2)}) async-start(), calls=%async_computation.14 | async-start | bytes 2359296 | tf_op jit(solution)/shard_map/all_gather | solution.py:9
  321.8 9.9 %copy-start.9 = (f32[256,512]{1,0:T(8,128)S(1)}, f32[256,512]{1,0:T(8,128)}, u32[]{:S(2)}) copy-start(f32[256,512]{1,0:T(8,128)} %param.31) | copy-start | bytes 1572868
  321.8 10.7 %copy-start.10 = (f32[256,512]{1,0:T(8,128)S(1)}, f32[256,512]{1,0:T(8,128)}, u32[]{:S(2)}) copy-start(f32[256,512]{1,0:T(8,128)} %param.30) | copy-start | bytes 1572868
  321.9 70.7 %all-gather.21.cloned.1.call-start = ((), (), s32[]{:S(2)}) async-start(), calls=%async_computation.8 | async-start | bytes 3932160 | tf_op jit(solution)/shard_map/all_gather | solution.py:51
  331.6 1.7 copy-start.16
  331.6 113.4 %all-gather.25.cloned.1.call-start = ((), (), s32[]{:S(2)}) async-start(), calls=%async_computation.10 | async-start | bytes 2359296 | tf_op jit(solution)/shard_map/all_gather | solution.py:85
  332.5 162.3 %all-gather.23.cloned.1.call-start = ((), (), s32[]{:S(2)}) async-start(), calls=%async_computation.9 | async-start | bytes 2359296 | tf_op jit(solution)/shard_map/all_gather | solution.py:84
  333.3 178.3 %reduce-scatter.6.cloned.1.call-start = ((), (), s32[]{:S(2)}) async-start(), calls=%async_computation.11 | async-start | bytes 3932160 | tf_op jit(solution)/shard_map/reduce_scatter | solution.py:57
  381.1 63.9 %copy-start.18 = (f32[2048]{0:T(1024)S(1)}, f32[2048]{0:T(1024)}, u32[]{:S(2)}) copy-start(f32[2048]{0:T(1024)} %param.22) | copy-start | bytes 24580
  381.2 63.9 %copy-start.22 = (f32[512]{0:T(512)S(1)}, f32[512]{0:T(512)}, u32[]{:S(2)}) copy-start(f32[512]{0:T(512)} %param.33) | copy-start | bytes 6148
  392.6 52.4 %copy-start.3 = (bf16[640,2048]{1,0:T(8,128)(2,1)S(1)}, bf16[640,2048]{1,0:T(8,128)(2,1)}, u32[]{:S(2)}) copy-start(bf16[640,2048]{1,0:T(8,128)(2,1)} %all-gather.21.cloned.1.call-done) | copy-start | bytes 7864324
  395.1 57.2 %copy-start.13 = (f32[512]{0:T(512)S(1)}, f32[512]{0:T(512)}, u32[]{:S(2)}) copy-start(f32[512]{0:T(512)} %param.35) | copy-start | bytes 6148
  395.1 57.2 %copy-start.14 = (f32[512]{0:T(512)S(1)}, f32[512]{0:T(512)}, u32[]{:S(2)}) copy-start(f32[512]{0:T(512)} %param.34) | copy-start | bytes 6148
  449.7 4.4 copy-start.11
  449.7 4.5 copy-start.12
  454.1 40.7 %copy-start.23 = (f32[512]{0:T(512)S(1)}, f32[512]{0:T(512)}, u32[]{:S(2)}) copy-start(f32[512]{0:T(512)} %param.32) | copy-start | bytes 6148
  502.5 9.0 %copy-start = (bf16[640,1024]{1,0:T(8,128)(2,1)S(1)}, bf16[640,1024]{1,0:T(8,128)(2,1)}, u32[]{:S(2)}) copy-start(bf16[640,1024]{1,0:T(8,128)(2,1)} %add_convert_fusion.2) | copy-start | bytes 3932164
  502.6 24.7 %all-gather.27.cloned.1.call-start = ((), (), s32[]{:S(2)}) async-start(), calls=%async_computation.12 | async-start | bytes 3932160 | tf_op jit(solution)/shard_map/all_gather | solution.py:51
  514.5 15.3 %copy-start.21 = (f32[2048]{0:T(1024)S(1)}, f32[2048]{0:T(1024)}, u32[]{:S(2)}) copy-start(f32[2048]{0:T(1024)} %param.23) | copy-start | bytes 24580
  514.5 51.0 %reduce-scatter.8.cloned.1.call-start = ((), (), s32[]{:S(2)}) async-start(), calls=%async_computation.13 | async-start | bytes 3932160 | tf_op jit(solution)/shard_map/reduce_scatter | solution.py:57
  527.3 2.5 copy-start.5
  553.8 11.6 %copy-start.1 = (bf16[640,1024]{1,0:T(8,128)(2,1)S(1)}, bf16[640,1024]{1,0:T(8,128)(2,1)}, u32[]{:S(2)}) copy-start(bf16[640,1024]{1,0:T(8,128)(2,1)} %add_convert_fusion.1) | copy-start | bytes 3932164
Sparse Core Ops, SparseCore 0:
  8.9 14.0 all-gather.12
  25.2 93.4 all-gather.14
  120.9 90.4 all-gather.16
  213.3 91.2 all-gather.18
  320.2 8.4 reduce-scatter.3
  330.7 50.4 all-gather.28
  382.7 9.8 all-gather.20
  394.7 50.2 all-gather.24
  447.2 47.6 all-gather.22
  502.7 8.8 reduce-scatter.5
  514.6 12.5 all-gather.26
  554.0 11.4 reduce-scatter.7
